TPU v7x, 32 devices: a whole 2x2x4 slice. The times are simulated.
32 devices in a mesh: ep: 8 (over z, x), tp: 4 (over y, core).
Axes of the slice: x: 2, y: 2, z: 4, core: 2. Of those that a mesh axis runs over, the one named last changes fastest.
Arguments:
- tokens: bfloat16 [1024, 2048], P('ep'), may hold values from -6 to 6
- chosen: int32 [8, 8, 7], P('ep'), may hold values from -1 to 127, as said below
- pick_weight: float32 [8, 8, 7], P('ep'), may hold values from 0.2 to 1
- gate_weight: bfloat16 [8, 2048, 4096], P('ep', None, 'tp'), may hold values from -0.125 to 0.125
- up_weight: bfloat16 [8, 2048, 4096], P('ep', None, 'tp'), may hold values from -0.125 to 0.125
- down_weight: bfloat16 [8, 4096, 2048], P('ep', 'tp'), may hold values from -0.09375 to 0.09375
Outputs:
- combined: bfloat16 [1024, 2048], P('ep', 'tp')
Inputs may be any that keep to these rules, and one draw needn't show every extreme that they name: `chosen`: within one group and one expert the named positions are distinct, and the filled slots come first. From each group every expert takes at least 3 tokens and at most 7; every expert takes exactly 7 tokens from some group, and exactly 40 tokens in all.
All inputs are finite; a program needn't handle non-finite values.
Results may differ from a plain program's by a relative error of at most 0.019.
Values may be sent and summed in bfloat16 or wider, within the bound.
No kernel may reach another device: no remote copies, remote signals or barrier semaphores. Data moves between devices by JAX's collectives and lax.ppermute only.
A program may use at most 64 MiB of HBM per device.

v0:
```python
import jax
import jax.numpy as jnp
from jax import lax
from jax.sharding import PartitionSpec as P


def on_device(tokens, chosen, pick_weight, gate_weight, up_weight, down_weight):
    model_width = tokens.shape[1]
    experts = chosen.shape[1]
    slot_count = chosen.shape[2]
    chosen_ids = chosen[0]
    filled = chosen_ids >= 0
    safe_ids = jnp.where(filled, chosen_ids, 0).reshape(-1)
    picked = jnp.take(tokens, safe_ids, axis=0)
    picked = jnp.where(filled.reshape(-1, 1), picked, jnp.zeros((), tokens.dtype))
    picked = picked.reshape(experts, slot_count, model_width)
    received = lax.all_to_all(picked, "ep", split_axis=0, concat_axis=0, tiled=True)
    expert_rows = received.reshape(-1, model_width)
    gate_pre = jnp.dot(expert_rows, gate_weight[0], preferred_element_type=jnp.float32)
    up_pre = jnp.dot(expert_rows, up_weight[0], preferred_element_type=jnp.float32)
    hidden = (jax.nn.silu(gate_pre) * up_pre).astype(jnp.bfloat16)
    down_local = down_weight[0]
    summed = lax.psum_scatter(
        jnp.einsum("fd,rf->dr", down_local, hidden, preferred_element_type=jnp.float32).astype(
            jnp.bfloat16
        ),
        "tp",
        scatter_dimension=0,
        tiled=True,
    )
    returned = lax.all_to_all(summed, "ep", split_axis=1, concat_axis=1, tiled=True)
    weights = jnp.where(filled, pick_weight[0], jnp.zeros((), jnp.float32)).reshape(-1)
    positions = lax.iota(jnp.int32, tokens.shape[0])
    onehot = jnp.where(
        positions[:, None] == safe_ids[None, :], weights[None, :], jnp.zeros((), jnp.float32)
    )
    combined = jnp.einsum(
        "tk,wk->tw",
        onehot,
        returned.astype(jnp.float32),
        precision=lax.Precision.HIGHEST,
        preferred_element_type=jnp.float32,
    )
    return combined.astype(jnp.bfloat16)


def solution(mesh):
    return jax.shard_map(
        on_device,
        mesh=mesh,
        in_specs=(
            P("ep", None),
            P("ep", None, None),
            P("ep", None, None),
            P("ep", None, "tp"),
            P("ep", None, "tp"),
            P("ep", "tp", None),
        ),
        out_specs=P("ep", "tp"),
        check_vma=False,
    )
```

profile of v0, /device:TPU:0, one launch (start us, length us, event | category | flops | bytes accessed | tf_op | source)
XLA Modules:
  0.0 74.2 jit_solution(4793843722620870495)
XLA Ops:
  6.5 0.0 copy-start
  6.5 0.0 reduce-scatter.2.cloned.1.call-start
  6.5 0.8 %copy.11 = s32[1,8,7]{2,1,0:T(8,128)S(1)} copy(s32[1,8,7]{1,0,2:T(1,128)} %param.7) | data formatting | bytes 448 | tf_op args[1]
  7.4 0.1 squeeze.22
  7.5 0.1 copy-done
  7.6 0.7 gather_fusion
  8.3 0.1 gather.7
  8.4 0.1 select_select_fusion
  8.5 16.0 %all_to_all.17 = bf16[8,7,2048]{2,1,0:T(8,128)(2,1)S(1)} all-to-all(bf16[8,7,2048]{2,1,0:T(8,128)(2,1)S(1)} %select_select_fusion), channel_id=1, replica_groups=mesh['ep'=8,'tp'=4] {'ep'}, dimensions={0} | all-to-all | bytes 458752 | tf_op jit(solution)/shard_map/all_to_all | solution.py:17
  24.5 0.1 reshape.74
  24.6 3.0 %fusion.4 = f32[56,1024]{1,0:T(8,128)S(1)} fusion(bf16[56,2048]{1,0:T(8,128)(2,1)S(1)} %reshape.74, bf16[1,2048,1024]{2,1,0:T(8,128)(2,1)} %param.9), kind=kOutput, calls=%fused_computation.5 | convolution fusion | flops 234881024 | bytes 4653056 | tf_op jit(solution)/shard_map/dot_general | solution.py:19
  27.6 0.0 copy-start.1
  27.6 5.7 %fusion.9 = bf16[2048,56]{0,1:T(8,128)(2,1)} fusion(bf16[1,1024,2048]{2,1,0:T(8,128)(2,1)} %param.11, bf16[56,2048]{1,0:T(8,128)(2,1)S(1)} %reshape.74, bf16[1,2048,1024]{2,1,0:T(8,128)(2,1)} %param.10, f32[56,1024]{1,0:T(8,128)S(1)} %fusion.4), kind=kOutput, calls=%fused_computation.8 | convolution fusion | flops 470220800 | bytes 9076736 | tf_op jit(solution)/shard_map/fd,rf->dr/dot_general | solution.py:24
  33.4 0.0 reduce-scatter.2.cloned.1.call-update
  33.4 0.1 squeeze.19
  33.5 0.0 copy-done.1
  33.5 0.1 copy.12
  33.5 0.1 squeeze.20
  33.6 18.9 %reduce-scatter.2.cloned.1.call-done = bf16[512,56]{0,1:T(8,128)(2,1)} async-done(((bf16[2048,56]{0,1:T(8,128)(2,1)}), bf16[512,56]{0,1:T(8,128)(2,1)}) %reduce-scatter.2.cloned.1.call-update) | async-done | bytes 57360 | tf_op jit(solution)/shard_map/reduce_scatter | solution.py:23
  52.5 1.5 %all_to_all.12 = bf16[512,8,7]{0,2,1:T(8,128)(2,1)} reshape(bf16[512,56]{0,1:T(8,128)(2,1)} %reduce-scatter.2.cloned.1.call-done) | data formatting | bytes 114688 | tf_op jit(solution)/shard_map/all_to_all | solution.py:31
  54.0 5.5 %all-to-all-start.1 = ((bf16[512,8,7]{0,2,1:T(8,128)(2,1)}), bf16[512,8,7]{0,2,1:T(8,128)(2,1)S(1)}, u32[]{:S(2)}, u32[]{:S(2)}) async-start(bf16[512,8,7]{0,2,1:T(8,128)(2,1)} %all_to_all.12), calls=%async_computation.2 | async-start | bytes 131072 | tf_op jit(solution)/shard_map/all_to_all | solution.py:31
  59.5 6.9 %all-to-all-done.1 = bf16[512,8,7]{0,2,1:T(8,128)(2,1)S(1)} async-done(((bf16[512,8,7]{0,2,1:T(8,128)(2,1)}), bf16[512,8,7]{0,2,1:T(8,128)(2,1)S(1)}, u32[]{:S(2)}, u32[]{:S(2)}) %all-to-all-start.1) | async-done | bytes 57376 | tf_op jit(solution)/shard_map/all_to_all | solution.py:31
  66.4 0.9 %convolution_convert_fusion = bf16[128,512]{1,0:T(8,128)(2,1)} fusion(bf16[512,56]{0,1:T(8,128)(2,1)S(1)} %all_to_all.14, f32[56]{0:T(128)S(1)} %compare_select_fusion.3, s32[56]{0:T(128)S(1)} %compare_select_fusion.4), kind=kOutput, calls=%fused_computation.10 | convolution fusion | flops 44120064 | bytes 188864 | tf_op jit(solution)/shard_map/tk,wk->tw/dot_general | solution.py:37
  (6 shorter events, 0.1 us)
Async XLA Ops:
  6.5 1.1 %copy-start = (bf16[128,2048]{1,0:T(8,128)(2,1)S(1)}, bf16[128,2048]{1,0:T(8,128)(2,1)}, u32[]{:S(2)}) copy-start(bf16[128,2048]{1,0:T(8,128)(2,1)} %param.6) | copy-start | bytes 1572868
  6.5 46.0 %reduce-scatter.2.cloned.1.call-start = ((), (), s32[]{:S(2)}) async-start(), calls=%async_computation.3 | async-start | bytes 286720 | tf_op jit(solution)/shard_map/reduce_scatter | solution.py:23
  27.6 5.8 %copy-start.1 = (f32[1,8,7]{1,0,2:T(1,128)S(1)}, f32[1,8,7]{1,0,2:T(1,128)}, u32[]{:S(2)}) copy-start(f32[1,8,7]{1,0,2:T(1,128)} %param.8) | copy-start | bytes 676
  54.0 12.4 %all-to-all-start.1 = ((bf16[512,8,7]{0,2,1:T(8,128)(2,1)}), bf16[512,8,7]{0,2,1:T(8,128)(2,1)S(1)}, u32[]{:S(2)}, u32[]{:S(2)}) async-start(bf16[512,8,7]{0,2,1:T(8,128)(2,1)} %all_to_all.12), calls=%async_computation.2 | async-start | bytes 131072 | tf_op jit(solution)/shard_map/all_to_all | solution.py:31
Sparse Core Ops, SparseCore 0:
  33.5 18.9 reduce-scatter.1
where the time goes:
time: 74.5 us; the launch traced here: 74.2 us
  waiting for transfers between devices  25.8 us (35%)
  blocking collectives  16 us (21%)
  between operations  13.4 us (18%)
  matrix products  9.65 us (13%)
  starting transfers between devices  5.5 us (7%)
  local copies, waits for them, and re-layouts  3.66 us (5%)
    reduce_scatter x1, waiting for transfers between devices, on_device(): lax.psum_scatter(jnp.einsum('fd,rf->dr', down_local, hidden, preferred_el...  18.9 us
    all_to_all x1, blocking collectives, on_device(): lax.all_to_all(picked, 'ep', split_axis=0, concat_axis=0, tiled=True)  16 us
    all_to_all x1, waiting for transfers between devices, on_device(): lax.all_to_all(summed, 'ep', split_axis=1, concat_axis=1, tiled=True)  6.9 us
    dot_general x1, matrix products, on_device(): jnp.einsum('fd,rf->dr', down_local, hidden, preferred_element_type=jnp.fl...  5.72 us
    all_to_all x1, starting transfers between devices, on_device(): lax.all_to_all(summed, 'ep', split_axis=1, concat_axis=1, tiled=True)  5.5 us
    dot_general x1, matrix products, on_device(): jnp.dot(expert_rows, gate_weight[0], preferred_element_type=jnp.float32)  3.02 us
    all_to_all x2, local copies, waits for them, and re-layouts, on_device(): lax.all_to_all(summed, 'ep', split_axis=1, concat_axis=1, tiled=True)  1.51 us
  transfers between devices with their start and end apart: 2, of which 2 were waited for; matrix products, arithmetic and copies ran while one was open for 0% of the time, Pallas kernels for 0%

commit v1 on v0

v1 whole, which is shorter than its diff:
```python
import jax
import jax.numpy as jnp
from jax import lax
from jax.sharding import PartitionSpec as P
PAD = 8
def first(tokens, chosen, n_tp):
    E = chosen.shape[1]; T = tokens.shape[0]
    ids = jnp.pad(chosen[0], ((0, 0), (0, PAD - chosen.shape[2])), constant_values=-1)
    oh = (ids.reshape(-1)[:, None] == lax.iota(jnp.int32, T)[None, :]).astype(jnp.bfloat16)
    picked = jnp.dot(oh, tokens, preferred_element_type=jnp.float32).astype(jnp.bfloat16)
    return ids, picked.reshape(E, PAD, -1)
def ffn(rows, gw, uw, dw):
    g = jnp.dot(rows, gw[0], preferred_element_type=jnp.float32)
    u = jnp.dot(rows, uw[0], preferred_element_type=jnp.float32)
    h = (jax.nn.silu(g) * u).astype(jnp.bfloat16)
    return jnp.dot(h, dw[0], preferred_element_type=jnp.float32).astype(jnp.bfloat16)
def weights(ids, pw, T):
    w = jnp.pad(pw[0], ((0, 0), (0, PAD - pw.shape[2])))
    return jnp.where(lax.iota(jnp.int32, T)[:, None, None] == ids[None], w[None], 0.0)
def perm_a2a(x, axis):
    n = lax.axis_size(axis)
    i = lax.axis_index(axis)
    parts = [None] * n
    outs = [lax.dynamic_index_in_dim(x, i, 0, keepdims=False)]
    for d in range(1, n):
        send = lax.dynamic_index_in_dim(x, (i + d) % n, 0, keepdims=False)
        outs.append(lax.ppermute(send, axis, [(s, (s + d) % n) for s in range(n)]))
    src = (i - jnp.arange(n)) % n
    return outs, src
def on_device(tokens, chosen, pw, gw, uw, dw):
    n_tp = lax.axis_size("tp")
    E = chosen.shape[1]; T = tokens.shape[0]; D = tokens.shape[1]
    F = D // n_tp
    ids, picked = first(tokens, chosen, n_tp)
    received = lax.all_to_all(picked, "ep", split_axis=0, concat_axis=0, tiled=True)
    rows = received.reshape(-1, D)
    part = ffn(rows, gw, uw, dw)
    p4 = part.reshape(E, PAD, n_tp, F).transpose(0, 2, 1, 3).reshape(E * n_tp, PAD, F)
    got = lax.all_to_all(p4, ("ep", "tp"), split_axis=0, concat_axis=0, tiled=True)
    w = weights(ids, pw, T)
    w = jnp.broadcast_to(w[:, :, None, :], (T, E, n_tp, PAD)).reshape(T, -1)
    return jnp.dot(w, got.reshape(-1, F).astype(jnp.float32), precision=lax.Precision.HIGHEST, preferred_element_type=jnp.float32).astype(jnp.bfloat16)
def solution(mesh):
    return jax.shard_map(on_device, mesh=mesh,
        in_specs=(P("ep", None), P("ep", None, None), P("ep", None, None), P("ep", None, "tp"), P("ep", None, "tp"), P("ep", "tp", None)),
        out_specs=P("ep", "tp"), check_vma=False)
```

time: 74.5 us -> 41.6 us (0.56)
  waiting for transfers between devices: 25.8 us -> 10.4 us
  between operations: 13.4 us -> 0.05 us
  local copies, waits for them, and re-layouts: 3.66 us -> 1.16 us
  starting transfers between devices: 5.5 us -> 3.63 us
    reduce_scatter x1 -> x0, waiting for transfers between devices: 18.9 us -> none  [on_device(): lax.psum_scatter(jnp.einsum('fd,rf->dr', down_local, hidden, preferred_el...]
    all_to_all x1, waiting for transfers between devices: 6.9 us -> 10.4 us  [on_device(): lax.all_to_all(p4, ('ep', 'tp'), split_axis=0, concat_axis=0, tiled=True)]
    all_to_all x1, starting transfers between devices: 5.5 us -> 3.63 us  [on_device(): lax.all_to_all(p4, ('ep', 'tp'), split_axis=0, concat_axis=0, tiled=True)]
    all_to_all x2 -> x0, local copies, waits for them, and re-layouts: 1.51 us -> none  [on_device(): lax.all_to_all(summed, 'ep', split_axis=1, concat_axis=1, tiled=True)]
    gather x2 -> x0, local copies, waits for them, and re-layouts: 0.8 us -> none  [on_device(): picked = jnp.take(tokens, safe_ids, axis=0)]
    dot_general x3 -> x4, matrix products: 9.65 us -> 10 us  [the longest x1 5.75 us: ffn(): jnp.dot(h, dw[0], preferred_element_type=jnp.float32).astype(jnp.bfloat16)]
  transfers between devices with their start and end apart: 2 -> 1, of which waited for: 2 -> 1; matrix products, arithmetic and copies ran while one was open for 0% -> 0% of each run, Pallas kernels for 0% -> 0%
where the time goes in v1:
time: 41.6 us; the launch traced here: 41.3 us
  blocking collectives  16 us (38%)
  waiting for transfers between devices  10.4 us (25%)
  matrix products  10 us (24%)
  starting transfers between devices  3.63 us (9%)
  local copies, waits for them, and re-layouts  1.16 us (3%)
    all_to_all x1, blocking collectives, on_device(): lax.all_to_all(picked, 'ep', split_axis=0, concat_axis=0, tiled=True)  16 us
    all_to_all x1, waiting for transfers between devices, on_device(): lax.all_to_all(p4, ('ep', 'tp'), split_axis=0, concat_axis=0, tiled=True)  10.4 us
    dot_general x1, matrix products, ffn(): jnp.dot(h, dw[0], preferred_element_type=jnp.float32).astype(jnp.bfloat16)  5.75 us
    all_to_all x1, starting transfers between devices, on_device(): lax.all_to_all(p4, ('ep', 'tp'), split_axis=0, concat_axis=0, tiled=True)  3.63 us
    dot_general x1, matrix products, ffn(): g = jnp.dot(rows, gw[0], preferred_element_type=jnp.float32)  3.02 us
    unnamed x6, local copies, waits for them, and re-layouts  1.06 us
    dot_general x1, matrix products, on_device(): jnp.dot(w, got.reshape(-1, F).astype(jnp.float32), precision=lax.Precisio...  0.98 us
  transfers between devices with their start and end apart: 1, of which 1 were waited for; matrix products, arithmetic and copies ran while one was open for 0% of the time, Pallas kernels for 0%

profile of v1, /device:TPU:0, one launch (start us, length us, event | category | flops | bytes accessed | tf_op | source)
XLA Modules:
  0.0 41.3 jit_solution(12767263981728551251)
XLA Ops:
  0.0 0.0 copy-start
  0.0 0.8 %copy.9 = s32[1,8,7]{2,1,0:T(8,128)S(1)} copy(s32[1,8,7]{1,0,2:T(1,128)} %param.7) | data formatting | bytes 448 | tf_op args[1]
  0.8 0.1 eq.35
  0.9 0.1 copy-done
  1.1 0.3 fusion.9
  1.3 16.0 %all_to_all.10 = bf16[8,8,2048]{2,1,0:T(8,128)(2,1)S(1)} all-to-all(bf16[8,8,2048]{2,1,0:T(8,128)(2,1)S(1)} %fusion.9), channel_id=1, replica_groups=mesh['ep'=8,'tp'=4] {'ep'}, dimensions={0} | all-to-all | bytes 524288 | tf_op jit(solution)/shard_map/all_to_all | solution.py:35
  17.3 3.0 %fusion.4 = f32[64,1024]{1,0:T(8,128)S(1)} fusion(bf16[1,2048,1024]{2,1,0:T(8,128)(2,1)} %param.9, bf16[8,8,2048]{2,1,0:T(8,128)(2,1)S(1)} %all_to_all.10), kind=kOutput, calls=%fused_computation.4 | convolution fusion | flops 268435456 | bytes 4718592 | tf_op jit(solution)/shard_map/dot_general | solution.py:13
  20.4 0.0 copy-start.1
  20.4 5.8 %fusion.6 = bf16[64,2048]{1,0:T(8,128)(2,1)} fusion(bf16[1,1024,2048]{2,1,0:T(8,128)(2,1)} %param.11, bf16[1,2048,1024]{2,1,0:T(8,128)(2,1)} %param.10, bf16[8,8,2048]{2,1,0:T(8,128)(2,1)S(1)} %all_to_all.10, f32[64,1024]{1,0:T(8,128)S(1)} %fusion.4), kind=kOutput, calls=%fused_computation.7 | convolution fusion | flops 537395200 | bytes 9175040 | tf_op jit(solution)/shard_map/dot_general | solution.py:16
  26.1 3.6 %all-to-all-start.1 = ((bf16[32,8,512]{2,1,0:T(8,128)(2,1)}), bf16[32,8,512]{2,1,0:T(8,128)(2,1)S(1)}, u32[]{:S(2)}, u32[]{:S(2)}) async-start(bf16[32,8,512]{2,1,0:T(8,128)(2,1)} %bitcast.10), calls=%async_computation.1 | async-start | bytes 524288 | tf_op jit(solution)/shard_map/all_to_all | solution.py:39
  29.8 0.0 copy-done.1
  29.8 0.1 copy.10
  29.9 0.1 fusion.28
  29.9 10.4 %all-to-all-done.1 = bf16[32,8,512]{2,1,0:T(8,128)(2,1)S(1)} async-done(((bf16[32,8,512]{2,1,0:T(8,128)(2,1)}), bf16[32,8,512]{2,1,0:T(8,128)(2,1)S(1)}, u32[]{:S(2)}, u32[]{:S(2)}) %all-to-all-start.1) | async-done | bytes 262176 | tf_op jit(solution)/shard_map/all_to_all | solution.py:39
  40.3 1.0 %convolution_convert_fusion.1 = bf16[128,512]{1,0:T(8,128)(2,1)} fusion(f32[128,256]{0,1:T(8,128)S(1)} %bitcast.38, bf16[32,8,512]{2,1,0:T(8,128)(2,1)S(1)} %all-to-all-done.1), kind=kOutput, calls=%fused_computation.11 | convolution fusion | flops 201392128 | bytes 524288 | tf_op jit(solution)/shard_map/dot_general | solution.py:42
  (3 shorter events, 0.0 us)
Async XLA Ops:
  0.0 1.1 %copy-start = (bf16[128,2048]{1,0:T(8,128)(2,1)S(1)}, bf16[128,2048]{1,0:T(8,128)(2,1)}, u32[]{:S(2)}) copy-start(bf16[128,2048]{1,0:T(8,128)(2,1)} %param.6) | copy-start | bytes 1572868
  20.4 9.4 %copy-start.1 = (f32[1,8,7]{1,0,2:T(1,128)S(1)}, f32[1,8,7]{1,0,2:T(1,128)}, u32[]{:S(2)}) copy-start(f32[1,8,7]{1,0,2:T(1,128)} %param.8) | copy-start | bytes 676
  26.1 14.2 %all-to-all-start.1 = ((bf16[32,8,512]{2,1,0:T(8,128)(2,1)}), bf16[32,8,512]{2,1,0:T(8,128)(2,1)S(1)}, u32[]{:S(2)}, u32[]{:S(2)}) async-start(bf16[32,8,512]{2,1,0:T(8,128)(2,1)} %bitcast.10), calls=%async_computation.1 | async-start | bytes 524288 | tf_op jit(solution)/shard_map/all_to_all | solution.py:39

commit v2 on v0

v2 whole, which is shorter than its diff:
```python
import jax
import jax.numpy as jnp
from jax import lax
from jax.experimental import pallas as pl
from jax.experimental.pallas import tpu as pltpu
from jax.sharding import PartitionSpec as P

SUB = 8
CHUNK = 512


def start_all(copies):
    for c in copies:
        c.start()


def half_copies(start, half, width, gate, up, gate_v, up_v, sem):
    n = gate_v.shape[0]
    copies = []
    for c in range(n):
        for k, (src, dst) in enumerate(((gate, gate_v), (up, up_v))):
            where = src.at[0, pl.ds(pl.multiple_of(start, 128), half), pl.ds(c * width, width)]
            copies.append(pltpu.make_async_copy(where, dst.at[c], sem.at[2 * c + k]))
    return copies


def own_body(rows, gate, up, g_out, u_out, gate_v, up_v, sem):
    n, half, width = gate_v.shape
    copies = half_copies(lax.axis_index("tp") % 2 * half, half, width, gate, up, gate_v, up_v, sem)
    start_all(copies)
    for c in range(n):
        cols = slice(c * width, (c + 1) * width)
        copies[2 * c].wait()
        g_out[:, cols] = jnp.dot(rows[...], gate_v[c], preferred_element_type=jnp.float32)
        copies[2 * c + 1].wait()
        u_out[:, cols] = jnp.dot(rows[...], up_v[c], preferred_element_type=jnp.float32)


def other_body(rows, g_in, u_in, gate, up, down, out, gate_v, up_v, down_v, hid, sem, sem_d):
    n, half, width = gate_v.shape
    n_out, _, width_out = down_v.shape
    copies = half_copies((1 - lax.axis_index("tp") % 2) * half, half, width, gate, up, gate_v, up_v, sem)
    copies_d = [
        pltpu.make_async_copy(down.at[0, :, pl.ds(c * width_out, width_out)], down_v.at[c], sem_d.at[c])
        for c in range(n_out)
    ]
    start_all(copies)
    start_all(copies_d)
    for c in range(n):
        cols = slice(c * width, (c + 1) * width)
        copies[2 * c].wait()
        g = g_in[:, cols] + jnp.dot(rows[...], gate_v[c], preferred_element_type=jnp.float32)
        copies[2 * c + 1].wait()
        u = u_in[:, cols] + jnp.dot(rows[...], up_v[c], preferred_element_type=jnp.float32)
        hid[:, cols] = (g / (1.0 + jnp.exp(-g)) * u).astype(hid.dtype)
    for c in range(n_out):
        copies_d[c].wait()
        out[:, c * width_out : (c + 1) * width_out] = jnp.dot(
            hid[...], down_v[c], preferred_element_type=jnp.float32).astype(out.dtype)


VMEM = pl.BlockSpec(memory_space=pltpu.VMEM)
HBM = pl.BlockSpec(memory_space=pl.ANY)


def own_half(rows, gate, up):
    m, half = rows.shape
    ff = gate.shape[2]
    width = min(CHUNK, ff)
    n = ff // width
    pre = pltpu.VMEM((m, ff), jnp.float32)
    return pl.pallas_call(
        own_body,
        out_shape=[pre, pre],
        in_specs=[VMEM, HBM, HBM],
        out_specs=[VMEM, VMEM],
        scratch_shapes=[
            pltpu.VMEM((n, half, width), gate.dtype),
            pltpu.VMEM((n, half, width), up.dtype),
            pltpu.SemaphoreType.DMA((2 * n,)),
        ],
        cost_estimate=pl.CostEstimate(flops=4 * m * half * ff, bytes_accessed=4 * half * ff, transcendentals=0),
    )(rows, gate, up)


def other_half(rows, g, u, gate, up, down):
    m, half = rows.shape
    ff, d = down.shape[1:]
    width = min(CHUNK, ff)
    n = ff // width
    width_out = min(CHUNK, d)
    n_out = d // width_out
    return pl.pallas_call(
        other_body,
        out_shape=jax.ShapeDtypeStruct((m, d), jnp.bfloat16),
        in_specs=[VMEM, VMEM, VMEM, HBM, HBM, HBM],
        out_specs=VMEM,
        scratch_shapes=[
            pltpu.VMEM((n, half, width), gate.dtype),
            pltpu.VMEM((n, half, width), up.dtype),
            pltpu.VMEM((n_out, ff, width_out), down.dtype),
            pltpu.VMEM((m, ff), jnp.bfloat16),
            pltpu.SemaphoreType.DMA((2 * n,)),
            pltpu.SemaphoreType.DMA((n_out,)),
        ],
    )(rows, g, u, gate, up, down)


def on_device(tokens, chosen, pick_weight, gate_weight, up_weight, down_weight):
    n_tp = lax.axis_size("tp")
    core = lax.axis_index("tp") % 2
    experts, slots = chosen.shape[1:]
    n_tok, d = tokens.shape
    width = d // n_tp
    half = d // 2
    pad = -slots % SUB
    size = slots + pad
    ids = jnp.pad(chosen[0], ((0, 0), (0, pad)), constant_values=-1)
    weight = jnp.pad(pick_weight[0], ((0, 0), (0, pad)))
    positions = lax.iota(jnp.int32, n_tok)
    onehot = (ids.reshape(-1)[:, None] == positions[None, :]).astype(tokens.dtype)
    mine = lax.dynamic_slice_in_dim(tokens, core * half, half, 1)
    picked = jnp.dot(onehot, mine, preferred_element_type=jnp.float32).astype(tokens.dtype)
    own = lax.all_to_all(picked.reshape(experts, size, half), "ep", split_axis=0, concat_axis=0, tiled=True)
    own = own.reshape(-1, half)
    other = lax.ppermute(own, "tp", [(s, s ^ 1) for s in range(n_tp)])
    own = pltpu.with_memory_space_constraint(own, pltpu.VMEM)
    other = pltpu.with_memory_space_constraint(other, pltpu.VMEM)
    g, u = own_half(own, gate_weight, up_weight)
    g = pltpu.with_memory_space_constraint(g, pltpu.VMEM)
    u = pltpu.with_memory_space_constraint(u, pltpu.VMEM)
    part = other_half(other, g, u, gate_weight, up_weight, down_weight)
    part = part.reshape(experts, size, n_tp, width).transpose(0, 2, 1, 3).reshape(experts * n_tp, size, width)
    got = lax.all_to_all(part, ("ep", "tp"), split_axis=0, concat_axis=0, tiled=True).reshape(-1, width)
    spread = jnp.where(positions[:, None, None] == ids[None], weight[None], jnp.zeros((), jnp.float32))
    spread = jnp.broadcast_to(spread[:, :, None, :], (n_tok, experts, n_tp, size)).reshape(n_tok, -1)
    combined = jnp.dot(spread, got.astype(jnp.float32), precision=lax.Precision.HIGHEST, preferred_element_type=jnp.float32)
    return combined.astype(jnp.bfloat16)


def solution(mesh):
    return jax.shard_map(
        on_device,
        mesh=mesh,
        in_specs=(P("ep", None), P("ep", None, None), P("ep", None, None), P("ep", None, "tp"), P("ep", None, "tp"), P("ep", "tp", None)),
        out_specs=P("ep", "tp"),
        check_vma=False,
    )
```

time: 74.5 us -> 38.1 us (0.51)
  waiting for transfers between devices: 25.8 us -> 10.4 us
  between operations: 13.4 us -> 0.07 us
  matrix products: 9.65 us -> 1.2 us
  Pallas kernels: 0 us -> 7.9 us
  starting transfers between devices: 5.5 us -> 2.6 us
  local copies, waits for them, and re-layouts: 3.66 us -> 1.16 us
  blocking collectives: 16 us -> 14.4 us
    reduce_scatter x1 -> x0, waiting for transfers between devices: 18.9 us -> none  [on_device(): lax.psum_scatter(jnp.einsum('fd,rf->dr', down_local, hidden, preferred_el...]
    dot_general x3 -> x2, matrix products: 9.65 us -> 1.2 us  [the longest x1 0.98 us: on_device(): jnp.dot(spread, got.astype(jnp.float32), precision=lax.Precision.HIGHEST,...]
    pallas_call x0 -> x2, Pallas kernels: none -> 7.9 us  [the longest x1 5.4 us: other_half(): pl.pallas_call(other_body, out_shape=jax.ShapeDtypeStruct((m, d), jnp.bfl...]
    all_to_all x1, waiting for transfers between devices: 6.9 us -> 10.4 us  [on_device(): lax.all_to_all(part, ('ep', 'tp'), split_axis=0, concat_axis=0, tiled=True)]
    all_to_all x1, starting transfers between devices: 5.5 us -> 2.6 us  [on_device(): lax.all_to_all(part, ('ep', 'tp'), split_axis=0, concat_axis=0, tiled=True)]
    all_to_all x1, blocking collectives: 16 us -> 14.4 us  [on_device(): lax.all_to_all(picked.reshape(experts, size, half), 'ep', split_axis=0, c...]
    all_to_all x2 -> x0, local copies, waits for them, and re-layouts: 1.51 us -> none  [on_device(): lax.all_to_all(summed, 'ep', split_axis=1, concat_axis=1, tiled=True)]
    gather x2 -> x0, local copies, waits for them, and re-layouts: 0.8 us -> none  [on_device(): picked = jnp.take(tokens, safe_ids, axis=0)]
  transfers between devices with their start and end apart: 2 -> 2, of which waited for: 2 -> 1; matrix products, arithmetic and copies ran while one was open for 0% -> 0% of each run, Pallas kernels for 0% -> 7%
where the time goes in v2:
time: 38.1 us; the launch traced here: 37.8 us
  blocking collectives  14.4 us (38%)
  waiting for transfers between devices  10.4 us (27%)
  Pallas kernels  7.9 us (21%)
  starting transfers between devices  2.6 us (7%)
  matrix products  1.2 us (3%)
  local copies, waits for them, and re-layouts  1.16 us (3%)
    all_to_all x1, blocking collectives, on_device(): lax.all_to_all(picked.reshape(experts, size, half), 'ep', split_axis=0, c...  14.4 us
    all_to_all x1, waiting for transfers between devices, on_device(): lax.all_to_all(part, ('ep', 'tp'), split_axis=0, concat_axis=0, tiled=True)  10.4 us
    pallas_call x1, Pallas kernels, other_half(): pl.pallas_call(other_body, out_shape=jax.ShapeDtypeStruct((m, d), jnp.bfl...  5.4 us
    all_to_all x1, starting transfers between devices, on_device(): lax.all_to_all(part, ('ep', 'tp'), split_axis=0, concat_axis=0, tiled=True)  2.6 us
    pallas_call x1, Pallas kernels, own_half(): pl.pallas_call(own_body, out_shape=[pre, pre], in_specs=[VMEM, HBM, HBM],...  2.5 us
    unnamed x6, local copies, waits for them, and re-layouts  1.06 us
    dot_general x1, matrix products, on_device(): jnp.dot(spread, got.astype(jnp.float32), precision=lax.Precision.HIGHEST,...  0.98 us
  transfers between devices with their start and end apart: 2, of which 1 were waited for; matrix products, arithmetic and copies ran while one was open for 0% of the time, Pallas kernels for 7%

profile of v2, /device:TPU:0, one launch (start us, length us, event | category | flops | bytes accessed | tf_op | source)
XLA Modules:
  0.0 37.8 jit_solution(6560200027517889319)
XLA Ops:
  0.0 0.0 copy-start
  0.0 0.8 %copy.9 = s32[1,8,7]{2,1,0:T(8,128)S(1)} copy(s32[1,8,7]{1,0,2:T(1,128)} %param.7) | data formatting | bytes 448 | tf_op args[1]
  0.8 0.1 eq.37
  0.9 0.1 copy-done
  1.1 0.2 fusion
  1.3 14.4 %all_to_all.10 = bf16[8,8,1024]{2,1,0:T(8,128)(2,1)S(1)} all-to-all(bf16[8,8,1024]{2,1,0:T(8,128)(2,1)S(1)} %fusion), channel_id=1, replica_groups=mesh['ep'=8,'tp'=4] {'ep'}, dimensions={0} | all-to-all | bytes 262144 | tf_op jit(solution)/shard_map/all_to_all | solution.py:124
  15.7 0.0 collective-permute-start
  15.7 2.5 %shard_map.64 = (f32[64,1024]{1,0:T(8,128)S(1)}, f32[64,1024]{1,0:T(8,128)S(1)}) custom-call(bf16[64,1024]{1,0:T(8,128)(2,1)S(1)} %bitcast.16, bf16[1,2048,1024]{2,1,0:T(8,128)(2,1)} %gate.3, bf16[1,2048,1024]{2,1,0:T(8,128)(2,1)} %up.3), custom_call_target="tpu_custom_call" | custom-call | flops 268435456 | bytes 4194304 | tf_op jit(solution)/shard_map/pallas_call | solution.py:72
  18.2 0.0 collective-permute-done.rows
  18.2 0.0 copy-start.1
  18.2 5.4 %shard_map.65 = bf16[64,2048]{1,0:T(8,128)(2,1)} custom-call(bf16[64,1024]{1,0:T(8,128)(2,1)S(1)} %collective-permute-done.rows, f32[64,1024]{1,0:T(8,128)S(1)} %get-tuple-element.7.g_in, f32[64,1024]{1,0:T(8,128)S(1)} %get-tuple-element.8.u_in, bf16[1,2048,1024]{2,1,0:T(8,128)(2,1)} %gate.3, bf16[1,2048,1024]{2,1,0:T(8,128)(2,1)} %up.3, ...), custom_call_target="tpu_custom_call" | custom-call | tf_op jit(solution)/shard_map/pallas_call | solution.py:93
  23.7 2.6 %all-to-all-start.1 = ((bf16[32,8,512]{2,1,0:T(8,128)(2,1)}), bf16[32,8,512]{2,1,0:T(8,128)(2,1)S(1)}, u32[]{:S(2)}, u32[]{:S(2)}) async-start(bf16[32,8,512]{2,1,0:T(8,128)(2,1)} %bitcast.17), calls=%async_computation.1 | async-start | bytes 524288 | tf_op jit(solution)/shard_map/all_to_all | solution.py:134
  26.3 0.0 copy-done.1
  26.3 0.1 copy.10
  26.4 0.1 fusion.3
  26.4 10.4 %all-to-all-done.1 = bf16[32,8,512]{2,1,0:T(8,128)(2,1)S(1)} async-done(((bf16[32,8,512]{2,1,0:T(8,128)(2,1)}), bf16[32,8,512]{2,1,0:T(8,128)(2,1)S(1)}, u32[]{:S(2)}, u32[]{:S(2)}) %all-to-all-start.1) | async-done | bytes 262176 | tf_op jit(solution)/shard_map/all_to_all | solution.py:134
  36.8 1.0 %convolution_convert_fusion = bf16[128,512]{1,0:T(8,128)(2,1)} fusion(f32[128,256]{0,1:T(8,128)S(1)} %bitcast.18, bf16[32,8,512]{2,1,0:T(8,128)(2,1)S(1)} %all-to-all-done.1), kind=kOutput, calls=%fused_computation | convolution fusion | flops 201392128 | bytes 524288 | tf_op jit(solution)/shard_map/dot_general | solution.py:137
  (3 shorter events, 0.0 us)
Async XLA Ops:
  0.0 1.1 %copy-start = (bf16[128,2048]{1,0:T(8,128)(2,1)S(1)}, bf16[128,2048]{1,0:T(8,128)(2,1)}, u32[]{:S(2)}) copy-start(bf16[128,2048]{1,0:T(8,128)(2,1)} %param.6) | copy-start | bytes 1572868
  15.7 2.5 %collective-permute-start = (bf16[64,1024]{1,0:T(8,128)(2,1)S(1)}, bf16[64,1024]{1,0:T(8,128)(2,1)S(1)}, u32[]{:S(2)}, u32[]{:S(2)}) collective-permute-start(bf16[64,1024]{1,0:T(8,128)(2,1)S(1)} %bitcast.15), channel_id=1, source_target_pairs={{0,1},{1,0},{2,3},{3,2},{4,5},{5,4},{6,7},{7,6},{8,9},{9,8},{10,11... | collective-permute-start | bytes 393224 | tf_op jit(solution)/shard_map/ppermute | solution.py:126
  18.2 8.0 %copy-start.1 = (f32[1,8,7]{1,0,2:T(1,128)S(1)}, f32[1,8,7]{1,0,2:T(1,128)}, u32[]{:S(2)}) copy-start(f32[1,8,7]{1,0,2:T(1,128)} %param.8) | copy-start | bytes 676
  23.7 13.2 %all-to-all-start.1 = ((bf16[32,8,512]{2,1,0:T(8,128)(2,1)}), bf16[32,8,512]{2,1,0:T(8,128)(2,1)S(1)}, u32[]{:S(2)}, u32[]{:S(2)}) async-start(bf16[32,8,512]{2,1,0:T(8,128)(2,1)} %bitcast.17), calls=%async_computation.1 | async-start | bytes 524288 | tf_op jit(solution)/shard_map/all_to_all | solution.py:134
